TPU v7x, 32 devices: a whole 2x2x4 slice. The times are simulated.
32 devices in a mesh: sp: 8 (over z, core), tp: 4 (over y, x).
Axes of the slice: x: 2, y: 2, z: 4, core: 2. Of those that a mesh axis runs over, the one named last changes fastest.
Arguments:
- query_rows: bfloat16 [2048, 2048], P('sp', 'tp'), may hold values from -1000 to 1000
- key_rows: bfloat16 [2048, 256], P('sp'), may hold values from -6 to 6
- value_rows: bfloat16 [2048, 256], P('sp'), may hold values from -6 to 6
- sink_logits: float32 [32], P('tp'), may hold values from 1 to 6
- out_weight: bfloat16 [2048, 2048], P('tp'), may hold values from -0.375 to 0.375
- stream_in: bfloat16 [2048, 2048], P('sp'), may hold values from -6 to 6
- norm_gain: float32 [2048], replicated, may hold values from 0.1 to 1.9
- routes: int32 [2048, 2], P('sp'), may hold values from 0 to 7, all different within a row; in each aligned block of 256 rows (0 to 255, 256 to 511, ...) at most 96 rows name the same one
- route_weights: float32 [2048, 2], P('sp'), may hold values from 0.2 to 1
- gate_weight: bfloat16 [8, 2048, 4096], P('sp', None, 'tp'), may hold values from -0.125 to 0.125
- up_weight: bfloat16 [8, 2048, 4096], P('sp', None, 'tp'), may hold values from -0.125 to 0.125
- down_weight: bfloat16 [8, 4096, 2048], P('sp', 'tp'), may hold values from -0.09375 to 0.09375
Outputs:
- layer_out: bfloat16 [2048, 2048], P(('sp', 'tp'))
Inputs may be any that keep to these rules, and one draw needn't show every extreme that they name: `routes`: each row names 2 different experts. Within the rows of one device (256 aligned rows) no expert is named more than 96 times, a bound that some block reaches.
All inputs are finite; a program needn't handle non-finite values.
Results may differ from a plain program's by a relative error of at most 0.015.
Values may be sent and summed in bfloat16 or wider, within the bound.
A program may use at most 64 MiB of HBM per device.

v0:
```python
import jax
import jax.numpy as jnp
from jax import lax
from jax.sharding import PartitionSpec as P

HEAD_DIM = 64
REP = 8
WINDOW = 128


norm_eps = 1e-06


def shifted(block, axis, distance):
    devices = range(lax.axis_size(axis))
    route = [(i - distance, i) for i in devices if i - distance in devices]
    return lax.ppermute(block, axis, route)


def rms_scale(stream, norm_gain):
    values = stream.astype(jnp.float32)
    scaled = values * lax.rsqrt(jnp.mean(values * values, axis=-1, keepdims=True) + norm_eps)
    return (scaled * norm_gain).astype(jnp.bfloat16)


def slot_tables(routes, experts_n, slot_cap):
    flat_ids = routes.reshape(-1)
    onehot = (flat_ids[:, None] == jnp.arange(experts_n, dtype=jnp.int32)[None, :]).astype(
        jnp.int32
    )
    before = jnp.cumsum(onehot, axis=0) - onehot
    targets = flat_ids * slot_cap + jnp.sum(before * onehot, axis=1)
    pair_token = jnp.arange(flat_ids.shape[0], dtype=jnp.int32) // routes.shape[1]
    slot_token = jnp.zeros((experts_n * slot_cap,), jnp.int32).at[targets].set(pair_token)
    slot_live = jnp.zeros((experts_n * slot_cap,), jnp.int32).at[targets].set(1)
    return (targets, slot_token, slot_live)


def per_device(
    query_rows,
    key_rows,
    value_rows,
    sink_logits,
    out_weight,
    stream_in,
    norm_gain,
    routes,
    route_weights,
    gate_weight,
    up_weight,
    down_weight,
):
    tok_count = query_rows.shape[0]
    local_heads = query_rows.shape[1] // HEAD_DIM
    tp_index = lax.axis_index("tp")
    kv_group = tp_index * local_heads // REP
    own_keys = lax.dynamic_slice_in_dim(key_rows, kv_group * HEAD_DIM, HEAD_DIM, 1)
    own_values = lax.dynamic_slice_in_dim(value_rows, kv_group * HEAD_DIM, HEAD_DIM, 1)
    prior_keys, prior_values = shifted(
        (own_keys[tok_count - WINDOW :], own_values[tok_count - WINDOW :]), "sp", 1
    )
    key_block = jnp.concatenate([prior_keys, own_keys], axis=0)
    value_block = jnp.concatenate([prior_values, own_values], axis=0)
    offset = lax.axis_index("sp") * tok_count
    query_pos = offset + jnp.arange(tok_count, dtype=jnp.int32)
    key_pos = offset - WINDOW + jnp.arange(tok_count + WINDOW, dtype=jnp.int32)
    distance = query_pos[:, None] - key_pos[None, :]
    allowed = (distance >= 0) & (distance < WINDOW) & (key_pos >= 0)[None, :]
    queries = query_rows.reshape(tok_count, local_heads, HEAD_DIM)
    scores = jnp.einsum(
        "qhd,kd->hqk", queries, key_block, preferred_element_type=jnp.float32
    ) * HEAD_DIM ** (-0.5)
    scores = jnp.where(allowed[None], scores, -1e30)
    sink_col = sink_logits.reshape(local_heads, 1, 1)
    row_peak = jnp.maximum(jnp.max(scores, axis=-1, keepdims=True), sink_col)
    exp_terms = jnp.exp(scores - row_peak)
    denom_sum = jnp.sum(exp_terms, axis=-1, keepdims=True) + jnp.exp(sink_col - row_peak)
    attn_probs = (exp_terms / denom_sum).astype(jnp.bfloat16)
    attended = jnp.einsum(
        "hqk,kd->qhd", attn_probs, value_block, preferred_element_type=jnp.float32
    )
    attended = attended.astype(jnp.bfloat16).reshape(tok_count, local_heads * HEAD_DIM)
    row_share = tok_count // lax.axis_size("tp")
    projected = lax.psum(
        jnp.dot(attended, out_weight, preferred_element_type=jnp.float32).astype(jnp.bfloat16), "tp"
    ).astype(jnp.float32)
    stream = (stream_in.astype(jnp.float32) + projected).astype(jnp.bfloat16)
    normed_all = rms_scale(stream, norm_gain)
    own_stream = lax.dynamic_slice_in_dim(stream, tp_index * row_share, row_share, 0)
    experts_n = lax.axis_size("sp")
    top_count = routes.shape[1]
    slot_cap = 3 * tok_count * top_count // (2 * experts_n)
    targets, slot_token, slot_live = slot_tables(routes, experts_n, slot_cap)
    width_share = normed_all.shape[1] // lax.axis_size("tp")
    columns = lax.dynamic_slice_in_dim(normed_all, tp_index * width_share, width_share, 1)
    outgoing = jnp.where(slot_live[:, None] > 0, columns[slot_token], jnp.zeros((), jnp.bfloat16))
    outgoing = outgoing.reshape(experts_n, slot_cap, width_share)
    arrived = lax.all_to_all(outgoing, "sp", split_axis=0, concat_axis=0, tiled=True)
    arrived = lax.all_gather(arrived, "tp", axis=2, tiled=True)
    sources = arrived.shape[0]
    item_count = arrived.shape[1]
    flat_rows = arrived.reshape(sources * item_count, arrived.shape[2])
    gate_act = jnp.dot(flat_rows, gate_weight[0], preferred_element_type=jnp.float32)
    up_act = jnp.dot(flat_rows, up_weight[0], preferred_element_type=jnp.float32)
    hidden = (jax.nn.silu(gate_act) * up_act).astype(jnp.bfloat16)
    partial_value = jnp.dot(hidden, down_weight[0], preferred_element_type=jnp.float32).astype(
        jnp.bfloat16
    )
    partial_value = partial_value.reshape(sources, item_count, partial_value.shape[1])
    returned = lax.all_to_all(partial_value, "sp", split_axis=0, concat_axis=0, tiled=True)
    returned_flat = returned.reshape(experts_n * slot_cap, returned.shape[2])
    pair_weights = route_weights.reshape(-1)
    chosen = returned_flat[targets].astype(jnp.float32) * pair_weights[:, None]
    moe_rows = lax.psum_scatter(
        jnp.sum(
            chosen.reshape(row_share * lax.axis_size("tp"), top_count, chosen.shape[1]), axis=1
        ).astype(jnp.bfloat16),
        "tp",
        scatter_dimension=0,
        tiled=True,
    ).astype(jnp.float32)
    return (own_stream.astype(jnp.float32) + moe_rows).astype(jnp.bfloat16)


def solution(mesh):
    return jax.shard_map(
        per_device,
        mesh=mesh,
        in_specs=(
            P("sp", "tp"),
            P("sp", None),
            P("sp", None),
            P("tp"),
            P("tp", None),
            P("sp", None),
            P(),
            P("sp", None),
            P("sp", None),
            P("sp", None, "tp"),
            P("sp", None, "tp"),
            P("sp", "tp", None),
        ),
        out_specs=P(("sp", "tp"), None),
        check_vma=False,
    )
```

profile of v0, /device:TPU:0, one launch (start us, length us, event | category | flops | bytes accessed | tf_op | source)
XLA Modules:
  0.0 299.9 jit_solution(17080001785737628045)
XLA Ops:
  6.5 1.1 constant_dynamic-slice_fusion
  7.7 2.4 collective-permute-start.1
  11.2 4.6 %collective-permute-start = (bf16[128,64]{0,1:T(8,128)(2,1)S(1)}, bf16[128,64]{0,1:T(8,128)(2,1)S(1)}, u32[]{:S(2)}, u32[]{:S(2)}) collective-permute-start(bf16[128,64]{0,1:T(8,128)(2,1)S(1)} %slice.20), channel_id=1, source_target_pairs={{0,4},{4,8},{8,12},{12,16},{16,20},{20,24},{24,28},{1,5},{5,9},{9,... | collective-permute-start | bytes 49160 | tf_op jit(solution)/shard_map/ppermute | solution.py:17
  17.7 1.1 copy.20
  18.8 1.1 reduce-window.6
  22.4 1.8 convolution_convert_fusion
  25.0 2.4 scatter_custom_fusion.1
  27.5 2.4 scatter_custom_fusion
  30.8 46.2 %all-reduce.2.cloned.1.call-done = bf16[256,2048]{1,0:T(8,128)(2,1)} async-done(((bf16[256,2048]{1,0:T(8,128)(2,1)}), bf16[256,2048]{1,0:T(8,128)(2,1)}) %all-reduce.2.cloned.1.call-update) | async-done | bytes 1048592 | tf_op jit(solution)/shard_map/psum | solution.py:84
  77.0 2.0 multiply_reduce_fusion.1
  79.5 3.3 %gather_fusion = bf16[768,512]{1,0:T(8,128)(2,1)} fusion(bf16[256,512]{1,0:T(8,128)(2,1)S(1)} %fusion.16, s32[1024]{0:T(1024)S(1)} %pad_clamp_fusion.1), kind=kCustom, calls=%fused_computation | custom fusion | bytes 1575936 | tf_op jit(solution)/shard_map/gather | solution.py:96
  82.8 1.3 broadcast_select_fusion
  84.1 25.5 %all_to_all.10 = bf16[8,96,512]{2,1,0:T(8,128)(2,1)} all-to-all(bf16[8,96,512]{2,1,0:T(8,128)(2,1)S(1)} %broadcast_select_fusion), channel_id=1, replica_groups=mesh['sp'=8,'tp'=4] {'sp'}, dimensions={0} | all-to-all | bytes 1572864 | tf_op jit(solution)/shard_map/all_to_all | solution.py:98
  109.6 41.8 %all-gather.2.cloned.1.call-done = bf16[8,96,2048]{2,1,0:T(8,128)(2,1)} async-done(((bf16[8,96,512]{2,1,0:T(8,128)(2,1)}), bf16[8,96,2048]{2,1,0:T(8,128)(2,1)}) %all-gather.2.cloned.1.call-update) | async-done | bytes 3145744 | tf_op jit(solution)/shard_map/all_gather | solution.py:99
  151.4 6.3 %fusion.2 = f32[768,1024]{1,0:T(8,128)S(1)} fusion(bf16[768,2048]{1,0:T(8,128)(2,1)} %bitcast.64, bf16[1,2048,1024]{2,1,0:T(8,128)(2,1)} %param.22), kind=kOutput, calls=%fused_computation.6 | convolution fusion | flops 3221225472 | bytes 10485760 | tf_op jit(solution)/shard_map/dot_general | solution.py:104
  157.7 3.8 %multiply_convert_fusion = bf16[768,1024]{1,0:T(8,128)(2,1)S(1)} fusion(f32[768,1024]{1,0:T(8,128)S(1)} %fusion.2, bf16[768,2048]{1,0:T(8,128)(2,1)S(1)} %bitcast.65, bf16[1,2048,1024]{2,1,0:T(8,128)(2,1)S(1)} %copy-done.3), kind=kOutput, calls=%fused_computation.13 | convolution fusion | flops 3225944064 | bytes 12058624 | tf_op jit(solution)/shard_map/dot_general | solution.py:103
  161.5 4.8 %fusion.6 = bf16[768,2048]{1,0:T(8,128)(2,1)} fusion(bf16[768,1024]{1,0:T(8,128)(2,1)S(1)} %multiply_convert_fusion, bf16[1,1024,2048]{2,1,0:T(8,128)(2,1)S(1)} %copy-done.4), kind=kOutput, calls=%fused_computation.11 | convolution fusion | flops 3222798336 | bytes 8912896 | tf_op jit(solution)/shard_map/dot_general | solution.py:106
  166.4 4.7 %all-to-all-start.1 = ((bf16[8,96,2048]{2,1,0:T(8,128)(2,1)}), bf16[8,96,2048]{2,1,0:T(8,128)(2,1)}, u32[]{:S(2)}, u32[]{:S(2)}) async-start(bf16[8,96,2048]{2,1,0:T(8,128)(2,1)} %bitcast.56), calls=%async_computation.1 | async-start | bytes 6291456 | tf_op jit(solution)/shard_map/all_to_all | solution.py:110
  171.5 71.2 %all-to-all-done.1 = bf16[8,96,2048]{2,1,0:T(8,128)(2,1)} async-done(((bf16[8,96,2048]{2,1,0:T(8,128)(2,1)}), bf16[8,96,2048]{2,1,0:T(8,128)(2,1)}, u32[]{:S(2)}, u32[]{:S(2)}) %all-to-all-start.1) | async-done | bytes 3145760 | tf_op jit(solution)/shard_map/all_to_all | solution.py:110
  242.7 7.6 %gather_fusion.1 = bf16[512,2048]{1,0:T(8,128)(2,1)} fusion(bf16[768,2048]{1,0:T(8,128)(2,1)} %bitcast.16, s32[1024]{0:T(1024)S(1)} %pad_clamp_fusion), kind=kCustom, calls=%fused_computation.1 | custom fusion | bytes 4196352 | tf_op jit(solution)/shard_map/gather | solution.py:113
  250.3 5.4 %reshape.209 = f32[256,2,2048]{2,1,0:T(2,128)} reshape(bf16[512,2048]{1,0:T(8,128)(2,1)} %gather_fusion.1) | data formatting | bytes 6291456 | tf_op jit(solution)/shard_map/convert_element_type | solution.py:113
  255.7 9.9 %multiply_reduce_fusion = bf16[256,2048]{1,0:T(8,128)(2,1)} fusion(f32[256,2,2048]{2,1,0:T(2,128)} %reshape.209, f32[256,2]{1,0:T(8,128)S(1)} %copy.25), kind=kLoop, calls=%fused_computation.10 | loop fusion | flops 1572864 | bytes 5244928 | tf_op jit(solution)/shard_map/reduce_sum | solution.py:115
  265.6 26.0 %reduce-scatter.2.cloned.1.call-done = bf16[64,2048]{1,0:T(8,128)(2,1)} async-done(((bf16[256,2048]{1,0:T(8,128)(2,1)}), bf16[64,2048]{1,0:T(8,128)(2,1)}) %reduce-scatter.2.cloned.1.call-update) | async-done | bytes 262160 | tf_op jit(solution)/shard_map/reduce_scatter | solution.py:114
  291.6 1.7 add_convert_fusion.1
  (58 shorter events, 7.9 us)
Async XLA Ops:
  6.5 15.9 %copy-start = (bf16[512,2048]{1,0:T(8,128)(2,1)S(1)}, bf16[512,2048]{1,0:T(8,128)(2,1)}, u32[]{:S(2)}) copy-start(bf16[512,2048]{1,0:T(8,128)(2,1)} %param.16) | copy-start | bytes 6291460
  6.5 14.0 %copy-start.2 = (f32[8]{0:T(128)S(1)}, f32[8]{0:T(128)}, u32[]{:S(2)}) copy-start(f32[8]{0:T(128)} %param.15) | copy-start | bytes 100
  6.5 70.5 %all-reduce.2.cloned.1.call-start = ((), (), s32[]{:S(2)}) async-start(), calls=%async_computation.3 | async-start | bytes 2097152 | tf_op jit(solution)/shard_map/psum | solution.py:84
  7.7 12.2 %collective-permute-start.1 = (bf16[128,64]{0,1:T(8,128)(2,1)S(1)}, bf16[128,64]{0,1:T(8,128)(2,1)S(1)}, u32[]{:S(2)}, u32[]{:S(2)}) collective-permute-start(bf16[128,64]{0,1:T(8,128)(2,1)S(1)} %slice.21), channel_id=1, source_target_pairs={{0,4},{4,8},{8,12},{12,16},{16,20},{20,24},{24,28},{1,5},{5,9},{9,... | collective-permute-start | bytes 49160 | tf_op jit(solution)/shard_map/ppermute | solution.py:17
  11.2 10.2 %collective-permute-start = (bf16[128,64]{0,1:T(8,128)(2,1)S(1)}, bf16[128,64]{0,1:T(8,128)(2,1)S(1)}, u32[]{:S(2)}, u32[]{:S(2)}) collective-permute-start(bf16[128,64]{0,1:T(8,128)(2,1)S(1)} %slice.20), channel_id=1, source_target_pairs={{0,4},{4,8},{8,12},{12,16},{16,20},{20,24},{24,28},{1,5},{5,9},{9,... | collective-permute-start | bytes 49160 | tf_op jit(solution)/shard_map/ppermute | solution.py:17
  24.2 127.2 %all-gather.2.cloned.1.call-start = ((), (), s32[]{:S(2)}) async-start(), calls=%async_computation.4 | async-start | bytes 3932160 | tf_op jit(solution)/shard_map/all_gather | solution.py:99
  151.4 6.3 %copy-start.3 = (bf16[1,2048,1024]{2,1,0:T(8,128)(2,1)S(1)}, bf16[1,2048,1024]{2,1,0:T(8,128)(2,1)}, u32[]{:S(2)}) copy-start(bf16[1,2048,1024]{2,1,0:T(8,128)(2,1)} %param.21) | copy-start | bytes 12582916
  151.4 6.3 %copy-start.5 = (bf16[8,96,2048]{2,1,0:T(8,128)(2,1)S(1)}, bf16[8,96,2048]{2,1,0:T(8,128)(2,1)}, u32[]{:S(2)}) copy-start(bf16[8,96,2048]{2,1,0:T(8,128)(2,1)} %all-gather.2.cloned.1.call-done) | copy-start | bytes 9437188
  157.7 3.8 %copy-start.4 = (bf16[1,1024,2048]{2,1,0:T(8,128)(2,1)S(1)}, bf16[1,1024,2048]{2,1,0:T(8,128)(2,1)}, u32[]{:S(2)}) copy-start(bf16[1,1024,2048]{2,1,0:T(8,128)(2,1)} %param.23) | copy-start | bytes 12582916
  166.4 5.0 %copy-start.1 = (f32[256,2]{0,1:T(2,128)S(1)}, f32[256,2]{0,1:T(2,128)}, u32[]{:S(2)}) copy-start(f32[256,2]{0,1:T(2,128)} %param.20) | copy-start | bytes 6148
  166.4 76.4 %all-to-all-start.1 = ((bf16[8,96,2048]{2,1,0:T(8,128)(2,1)}), bf16[8,96,2048]{2,1,0:T(8,128)(2,1)}, u32[]{:S(2)}, u32[]{:S(2)}) async-start(bf16[8,96,2048]{2,1,0:T(8,128)(2,1)} %bitcast.56), calls=%async_computation.1 | async-start | bytes 6291456 | tf_op jit(solution)/shard_map/all_to_all | solution.py:110
  171.1 120.5 %reduce-scatter.2.cloned.1.call-start = ((), (), s32[]{:S(2)}) async-start(), calls=%async_computation.5 | async-start | bytes 1310720 | tf_op jit(solution)/shard_map/reduce_scatter | solution.py:114
Sparse Core Ops, SparseCore 0:
  24.3 52.6 all-reduce.1
  109.7 41.6 all-gather.1
  265.7 25.8 reduce-scatter.1
where the time goes:
time: 301 us; the launch traced here: 300 us
  waiting for transfers between devices  185 us (61%)
  local copies, waits for them, and re-layouts  27.1 us (9%)
  blocking collectives  25.5 us (8%)
  other arithmetic  18.3 us (6%)
  matrix products  18.3 us (6%)
  between operations  13.4 us (4%)
  starting transfers between devices  12 us (4%)
    all_to_all x1, waiting for transfers between devices, per_device(): lax.all_to_all(partial_value, 'sp', split_axis=0, concat_axis=0, tiled=True)  71.2 us
    psum x1, waiting for transfers between devices, per_device(): lax.psum(jnp.dot(attended, out_weight, preferred_element_type=jnp.float32...  46.2 us
    all_gather x1, waiting for transfers between devices, per_device(): arrived = lax.all_gather(arrived, 'tp', axis=2, tiled=True)  41.8 us
    reduce_scatter x1, waiting for transfers between devices, per_device(): lax.psum_scatter(jnp.sum(chosen.reshape(row_share * lax.axis_size('tp'),...  26 us
    all_to_all x1, blocking collectives, per_device(): lax.all_to_all(outgoing, 'sp', split_axis=0, concat_axis=0, tiled=True)  25.5 us
    reduce_sum x1, other arithmetic, per_device(): jnp.sum(chosen.reshape(row_share * lax.axis_size('tp'), top_count, chosen...  9.87 us
    gather x1, local copies, waits for them, and re-layouts, per_device(): chosen = returned_flat[targets].astype(jnp.float32) * pair_weights[:, None]  7.56 us
    ppermute x2, starting transfers between devices, shifted(): return lax.ppermute(block, axis, route)  6.98 us
  transfers between devices with their start and end apart: 6, of which 4 were waited for; matrix products, arithmetic and copies ran while one was open for 4% of the time, Pallas kernels for 0%

commit v1 on v0

v1 whole, which is shorter than its diff:
```python
import functools

import jax
import jax.numpy as jnp
from jax import lax
from jax.experimental import pallas as pl
from jax.experimental.pallas import tpu as pltpu
from jax.sharding import PartitionSpec as P

HEAD_DIM = 64
REP = 8
WINDOW = 128
MESH = pl.DeviceIdType.MESH

norm_eps = 1e-06


def shifted(block, axis, distance):
    devices = range(lax.axis_size(axis))
    route = [(i - distance, i) for i in devices if i - distance in devices]
    return lax.ppermute(block, axis, route)


def slot_targets(routes, experts_n, slot_cap):
    flat_ids = routes.reshape(-1)
    onehot = (flat_ids[:, None] == jnp.arange(experts_n, dtype=jnp.int32)[None, :]).astype(
        jnp.int32
    )
    before = jnp.cumsum(onehot, axis=0) - onehot
    targets = flat_ids * slot_cap + jnp.sum(before * onehot, axis=1)
    return targets.reshape(routes.shape)


def greet(n_sp, n_tp, sp, tp):
    barrier = pltpu.get_barrier_semaphore()
    for d in range(1, n_tp):
        pl.semaphore_signal(
            barrier, inc=1, device_id=(sp, lax.rem(tp + d, n_tp)), device_id_type=MESH
        )
    for d in range(1, n_sp):
        pl.semaphore_signal(
            barrier, inc=1, device_id=(lax.rem(sp + d, n_sp), tp), device_id_type=MESH
        )
    pl.semaphore_wait(barrier, n_tp + n_sp - 2)


def remote(src, dst, send, recv, device):
    return pltpu.make_async_remote_copy(
        src_ref=src,
        dst_ref=dst,
        send_sem=send,
        recv_sem=recv,
        device_id=device,
        device_id_type=MESH,
    )


def front_kernel(
    n_sp,
    n_tp,
    part,
    stream_in,
    gain,
    slots_row,
    arrived,
    stream_out,
    recv,
    squares,
    squares_in,
    outgoing,
    rs_send,
    rs_recv,
    sq_send,
    sq_recv,
    a2a_send,
    a2a_recv,
    ag_send,
    ag_recv,
):
    sp = lax.axis_index("sp")
    tp = lax.axis_index("tp")
    width = recv.shape[2]
    depth = part.shape[1]
    cap = arrived.shape[1]
    tok = part.shape[0]
    top = slots_row.shape[0]
    mine = pl.ds(pl.multiple_of(tp * width, width), width)
    greet(n_sp, n_tp, sp, tp)

    copies = []
    for d in range(1, n_tp):
        peer = lax.rem(tp + d, n_tp)
        cols = pl.ds(pl.multiple_of(peer * width, width), width)
        c = remote(
            part.at[:, cols], recv.at[d - 1], rs_send.at[d - 1], rs_recv.at[d - 1], (sp, peer)
        )
        c.start()
        copies.append(c)
    total = part[:, mine].astype(jnp.float32)
    for d in range(1, n_tp):
        copies[d - 1].wait_recv()
        total = total + recv[d - 1].astype(jnp.float32)
    stream = (stream_in[:, mine].astype(jnp.float32) + total).astype(jnp.bfloat16)
    stream_out[...] = stream
    values = stream.astype(jnp.float32)
    row_sum = jnp.sum(values * values, axis=1, keepdims=True)
    spread = jnp.transpose(jnp.broadcast_to(row_sum, (tok, 128)))
    squares[...] = spread[0:8]
    sq_copies = []
    for d in range(1, n_tp):
        peer = lax.rem(tp + d, n_tp)
        c = remote(squares, squares_in.at[d - 1], sq_send.at[d - 1], sq_recv.at[d - 1], (sp, peer))
        c.start()
        sq_copies.append(c)
    full = spread[0:8]
    for d in range(1, n_tp):
        sq_copies[d - 1].wait_recv()
        full = full + squares_in[d - 1]
    scale = lax.rsqrt(full / depth + norm_eps)
    scale = jnp.transpose(jnp.broadcast_to(scale[0:1], (128, tok)))[:, 0:1]
    normed = (values * scale * gain[:, mine]).astype(jnp.bfloat16)

    def picked(j):
        want = lax.broadcasted_iota(jnp.int32, (cap, tok), 0) + j * cap
        hit = want == slots_row[0:1, :]
        for k in range(1, top):
            hit = hit | (want == slots_row[k : k + 1, :])
        onehot = jnp.where(hit, 1.0, 0.0).astype(jnp.bfloat16)
        return jnp.dot(onehot, normed, preferred_element_type=jnp.float32).astype(jnp.bfloat16)

    a2a = []
    for d in range(1, n_sp):
        j = lax.rem(sp + d, n_sp)
        outgoing[d - 1] = picked(j)
        a2a.append(
            remote(
                outgoing.at[d - 1],
                arrived.at[sp, :, mine],
                a2a_send.at[d - 1],
                a2a_recv.at[d - 1],
                (j, tp),
            )
        )
        if d > 1:
            a2a[d - 2].start()
    arrived[sp, :, mine] = picked(sp)
    a2a[-1].start()
    gathers = []
    for d in range(n_sp):
        source = lax.rem(sp + n_sp - d, n_sp)
        if d > 0:
            a2a[d - 1].wait_recv()
        block = arrived.at[source, :, mine]
        for q in range(1, n_tp):
            peer = lax.rem(tp + q, n_tp)
            c = remote(block, block, ag_send.at[q - 1, d], ag_recv.at[q - 1, d], (sp, peer))
            c.start()
            gathers.append(c)
    for c in gathers:
        c.wait_recv()
    for c in copies + sq_copies + a2a + gathers:
        c.wait_send()


def back_kernel(
    n_sp,
    n_tp,
    part,
    slots,
    weights,
    stream,
    out,
    recv,
    summed,
    returned,
    joined,
    rs_send,
    rs_recv,
    a2a_send,
    a2a_recv,
    last_send,
    last_recv,
):
    sp = lax.axis_index("sp")
    tp = lax.axis_index("tp")
    width = recv.shape[3]
    cap = part.shape[1]
    tok = stream.shape[0]
    rows = out.shape[0]
    top = slots.shape[1]
    mine = pl.ds(pl.multiple_of(tp * width, width), width)
    greet(n_sp, n_tp, sp, tp)

    order = list(range(1, n_sp)) + [0]
    reduce = {}
    for d in order:
        s = lax.rem(sp + d, n_sp)
        for q in range(1, n_tp):
            peer = lax.rem(tp + q, n_tp)
            cols = pl.ds(pl.multiple_of(peer * width, width), width)
            c = remote(
                part.at[s, :, cols],
                recv.at[q - 1, d],
                rs_send.at[q - 1, d],
                rs_recv.at[q - 1, d],
                (sp, peer),
            )
            c.start()
            reduce[q, d] = c

    def added(d):
        s = lax.rem(sp + d, n_sp)
        total = part[s, :, mine].astype(jnp.float32)
        for q in range(1, n_tp):
            reduce[q, d].wait_recv()
            total = total + recv[q - 1, d].astype(jnp.float32)
        return total.astype(jnp.bfloat16)

    a2a = []
    for d in range(1, n_sp):
        s = lax.rem(sp + d, n_sp)
        summed[d - 1] = added(d)
        a2a.append(
            remote(
                summed.at[d - 1],
                returned.at[d - 1],
                a2a_send.at[d - 1],
                a2a_recv.at[d - 1],
                (s, tp),
            )
        )
        if d > 1:
            a2a[d - 2].start()
    a2a[-1].start()

    def taken(expert, block):
        want = lax.broadcasted_iota(jnp.int32, (tok, cap), 1) + expert * cap
        gives = None
        for k in range(top):
            onehot = jnp.where(want == slots[:, k : k + 1], 1.0, 0.0).astype(jnp.bfloat16)
            term = jnp.dot(onehot, block, preferred_element_type=jnp.float32)
            term = term * weights[:, k : k + 1]
            gives = term if gives is None else gives + term
        return gives

    moe = taken(sp, added(0))
    for d in range(1, n_sp):
        a2a[d - 1].wait_recv()
        moe = moe + taken(lax.rem(sp + n_sp - d, n_sp), returned[d - 1])
    joined[...] = (stream[...].astype(jnp.float32) + moe).astype(jnp.bfloat16)
    last = []
    for q in range(1, n_tp):
        peer = lax.rem(tp + q, n_tp)
        there = pl.ds(pl.multiple_of(peer * rows, rows), rows)
        c = remote(
            joined.at[there], out.at[:, mine], last_send.at[q - 1], last_recv.at[q - 1], (sp, peer)
        )
        c.start()
        last.append(c)
    out[:, mine] = joined[pl.ds(pl.multiple_of(tp * rows, rows), rows), :]
    for c in last:
        c.wait_recv()
    for c in list(reduce.values()) + a2a + last:
        c.wait_send()


def vmem(count):
    return [pl.BlockSpec(memory_space=pltpu.VMEM)] * count


def per_device(
    query_rows,
    key_rows,
    value_rows,
    sink_logits,
    out_weight,
    stream_in,
    norm_gain,
    routes,
    route_weights,
    gate_weight,
    up_weight,
    down_weight,
):
    n_sp = lax.axis_size("sp")
    n_tp = lax.axis_size("tp")
    tok_count = query_rows.shape[0]
    local_heads = query_rows.shape[1] // HEAD_DIM
    tp_index = lax.axis_index("tp")
    kv_group = tp_index * local_heads // REP
    own_keys = lax.dynamic_slice_in_dim(key_rows, kv_group * HEAD_DIM, HEAD_DIM, 1)
    own_values = lax.dynamic_slice_in_dim(value_rows, kv_group * HEAD_DIM, HEAD_DIM, 1)
    prior_keys, prior_values = shifted(
        (own_keys[tok_count - WINDOW :], own_values[tok_count - WINDOW :]), "sp", 1
    )
    key_block = jnp.concatenate([prior_keys, own_keys], axis=0)
    value_block = jnp.concatenate([prior_values, own_values], axis=0)
    offset = lax.axis_index("sp") * tok_count
    query_pos = offset + jnp.arange(tok_count, dtype=jnp.int32)
    key_pos = offset - WINDOW + jnp.arange(tok_count + WINDOW, dtype=jnp.int32)
    distance = query_pos[:, None] - key_pos[None, :]
    allowed = (distance >= 0) & (distance < WINDOW) & (key_pos >= 0)[None, :]
    queries = query_rows.reshape(tok_count, local_heads, HEAD_DIM)
    scores = jnp.einsum(
        "qhd,kd->hqk", queries, key_block, preferred_element_type=jnp.float32
    ) * HEAD_DIM ** (-0.5)
    scores = jnp.where(allowed[None], scores, -1e30)
    sink_col = sink_logits.reshape(local_heads, 1, 1)
    row_peak = jnp.maximum(jnp.max(scores, axis=-1, keepdims=True), sink_col)
    exp_terms = jnp.exp(scores - row_peak)
    denom_sum = jnp.sum(exp_terms, axis=-1, keepdims=True) + jnp.exp(sink_col - row_peak)
    attn_probs = (exp_terms / denom_sum).astype(jnp.bfloat16)
    attended = jnp.einsum(
        "hqk,kd->qhd", attn_probs, value_block, preferred_element_type=jnp.float32
    )
    attended = attended.astype(jnp.bfloat16).reshape(tok_count, local_heads * HEAD_DIM)
    projected = jnp.dot(attended, out_weight, preferred_element_type=jnp.float32).astype(
        jnp.bfloat16
    )

    depth = stream_in.shape[1]
    width = depth // n_tp
    row_share = tok_count // n_tp
    top_count = routes.shape[1]
    slot_cap = 3 * tok_count * top_count // (2 * n_sp)
    targets = slot_targets(routes, n_sp, slot_cap)
    bf16 = jnp.bfloat16
    dma = pltpu.SemaphoreType.DMA
    arrived, stream = pl.pallas_call(
        functools.partial(front_kernel, n_sp, n_tp),
        out_shape=(
            jax.ShapeDtypeStruct((n_sp, slot_cap, depth), bf16),
            jax.ShapeDtypeStruct((tok_count, width), bf16),
        ),
        in_specs=vmem(4),
        out_specs=tuple(vmem(2)),
        scratch_shapes=[
            pltpu.VMEM((n_tp - 1, tok_count, width), bf16),
            pltpu.VMEM((8, tok_count), jnp.float32),
            pltpu.VMEM((n_tp - 1, 8, tok_count), jnp.float32),
            pltpu.VMEM((n_sp - 1, slot_cap, width), bf16),
            dma((n_tp - 1,)),
            dma((n_tp - 1,)),
            dma((n_tp - 1,)),
            dma((n_tp - 1,)),
            dma((n_sp - 1,)),
            dma((n_sp - 1,)),
            dma((n_tp - 1, n_sp)),
            dma((n_tp - 1, n_sp)),
        ],
        compiler_params=pltpu.CompilerParams(
            collective_id=0, has_side_effects=True, vmem_limit_bytes=32 << 20
        ),
        name="front",
    )(projected, stream_in, norm_gain.reshape(1, depth), jnp.transpose(targets))
    flat_rows = arrived.reshape(n_sp * slot_cap, depth)
    gate_act = jnp.dot(flat_rows, gate_weight[0], preferred_element_type=jnp.float32)
    up_act = jnp.dot(flat_rows, up_weight[0], preferred_element_type=jnp.float32)
    hidden = (jax.nn.silu(gate_act) * up_act).astype(bf16)
    partial_value = jnp.dot(hidden, down_weight[0], preferred_element_type=jnp.float32).astype(bf16)
    partial_value = partial_value.reshape(n_sp, slot_cap, depth)
    return pl.pallas_call(
        functools.partial(back_kernel, n_sp, n_tp),
        out_shape=jax.ShapeDtypeStruct((row_share, depth), bf16),
        in_specs=vmem(4),
        out_specs=vmem(1)[0],
        scratch_shapes=[
            pltpu.VMEM((n_tp - 1, n_sp, slot_cap, width), bf16),
            pltpu.VMEM((n_sp - 1, slot_cap, width), bf16),
            pltpu.VMEM((n_sp - 1, slot_cap, width), bf16),
            pltpu.VMEM((tok_count, width), bf16),
            dma((n_tp - 1, n_sp)),
            dma((n_tp - 1, n_sp)),
            dma((n_sp - 1,)),
            dma((n_sp - 1,)),
            dma((n_tp - 1,)),
            dma((n_tp - 1,)),
        ],
        compiler_params=pltpu.CompilerParams(
            collective_id=1, has_side_effects=True, vmem_limit_bytes=32 << 20
        ),
        name="back",
    )(partial_value, targets, route_weights, stream)


def solution(mesh):
    return jax.shard_map(
        per_device,
        mesh=mesh,
        in_specs=(
            P("sp", "tp"),
            P("sp", None),
            P("sp", None),
            P("tp"),
            P("tp", None),
            P("sp", None),
            P(),
            P("sp", None),
            P("sp", None),
            P("sp", None, "tp"),
            P("sp", None, "tp"),
            P("sp", "tp", None),
        ),
        out_specs=P(("sp", "tp"), None),
        check_vma=False,
    )
```

time: 301 us -> 133 us (0.44)
  waiting for transfers between devices: 185 us -> 0.01 us
  Pallas kernels: 0 us -> 102 us
  blocking collectives: 25.5 us -> 0 us
  local copies, waits for them, and re-layouts: 27.1 us -> 6.95 us
  other arithmetic: 18.3 us -> 2.97 us
  between operations: 13.4 us -> 0.29 us
  starting transfers between devices: 12 us -> 6.98 us
  matrix products: 18.3 us -> 13.5 us
    pallas_call x0 -> x2, Pallas kernels: none -> 102 us  [the longest x1 56.9 us: per_device(): pl.pallas_call(functools.partial(front_kernel, n_sp, n_tp), out_shape=(ja...]
    all_to_all x1 -> x0, waiting for transfers between devices: 71.2 us -> none  [per_device(): lax.all_to_all(partial_value, 'sp', split_axis=0, concat_axis=0, tiled=True)]
    psum x1 -> x0, waiting for transfers between devices: 46.2 us -> none  [per_device(): lax.psum(jnp.dot(attended, out_weight, preferred_element_type=jnp.float32...]
    all_gather x1 -> x0, waiting for transfers between devices: 41.8 us -> none  [per_device(): arrived = lax.all_gather(arrived, 'tp', axis=2, tiled=True)]
    reduce_scatter x1 -> x0, waiting for transfers between devices: 26 us -> none  [per_device(): lax.psum_scatter(jnp.sum(chosen.reshape(row_share * lax.axis_size('tp'),...]
    all_to_all x1 -> x0, blocking collectives: 25.5 us -> none  [per_device(): lax.all_to_all(outgoing, 'sp', split_axis=0, concat_axis=0, tiled=True)]
    reduce_sum x3 -> x1, other arithmetic: 12 us -> 0.09 us  [slot_targets(): targets = flat_ids * slot_cap + jnp.sum(before * onehot, axis=1)]
    gather x2 -> x0, local copies, waits for them, and re-layouts: 10.9 us -> none  [the longest x1 7.56 us: per_device(): chosen = returned_flat[targets].astype(jnp.float32) * pair_weights[:, None]]
  transfers between devices with their start and end apart: 6 -> 2, of which waited for: 4 -> 0; matrix products, arithmetic and copies ran while one was open for 4% -> 6% of each run, Pallas kernels for 0% -> 0%
where the time goes in v1:
time: 133 us
  Pallas kernels  102 us (77%)
  matrix products  13.5 us (10%)
  starting transfers between devices  6.98 us (5%)
  local copies, waits for them, and re-layouts  6.95 us (5%)
  other arithmetic  2.97 us (2%)
    pallas_call x1, Pallas kernels, per_device(): pl.pallas_call(functools.partial(front_kernel, n_sp, n_tp), out_shape=(ja...  56.9 us
    pallas_call x1, Pallas kernels, per_device(): pl.pallas_call(functools.partial(back_kernel, n_sp, n_tp), out_shape=jax....  45.4 us
    ppermute x2, starting transfers between devices, shifted(): return lax.ppermute(block, axis, route)  6.98 us
    unnamed x20, local copies, waits for them, and re-layouts  4.08 us
    dot_general x1, matrix products, per_device(): jnp.dot(hidden, down_weight[0], preferred_element_type=jnp.float32)  3.82 us
    dot_general x1, matrix products, per_device(): jnp.dot(flat_rows, gate_weight[0], preferred_element_type=jnp.float32)  3.81 us
    dot_general x1, matrix products, per_device(): jnp.dot(flat_rows, up_weight[0], preferred_element_type=jnp.float32)  3.49 us
  transfers between devices with their start and end apart: 2, of which 0 were waited for; matrix products, arithmetic and copies ran while one was open for 6% of the time, Pallas kernels for 0%

profile of v1, /device:TPU:0, one launch (start us, length us, event | category | flops | bytes accessed | tf_op | source)
XLA Modules:
  0.0 133.0 jit_solution(9020518382338342906)
XLA Ops:
  0.0 1.1 constant_dynamic-slice_fusion
  1.2 2.4 %collective-permute-start.1 = (bf16[128,64]{0,1:T(8,128)(2,1)S(1)}, bf16[128,64]{0,1:T(8,128)(2,1)S(1)}, u32[]{:S(2)}, u32[]{:S(2)}) collective-permute-start(bf16[128,64]{0,1:T(8,128)(2,1)S(1)} %slice.17), channel_id=1, source_target_pairs={{0,4},{4,8},{8,12},{12,16},{16,20},{20,24},{24,28},{1,5},{5,9},{9,... | collective-permute-start | bytes 49160 | tf_op jit(solution)/shard_map/ppermute | solution.py:21
  3.6 0.9 constant_dynamic-slice_fusion.1
  4.7 4.6 %collective-permute-start = (bf16[128,64]{0,1:T(8,128)(2,1)S(1)}, bf16[128,64]{0,1:T(8,128)(2,1)S(1)}, u32[]{:S(2)}, u32[]{:S(2)}) collective-permute-start(bf16[128,64]{0,1:T(8,128)(2,1)S(1)} %slice.16), channel_id=1, source_target_pairs={{0,4},{4,8},{8,12},{12,16},{16,20},{20,24},{24,28},{1,5},{5,9},{9,... | collective-permute-start | bytes 49160 | tf_op jit(solution)/shard_map/ppermute | solution.py:21
  9.3 0.8 copy.35
  10.1 0.1 eq.29
  10.3 0.1 eq.25
  10.4 0.7 broadcast_multiply_fusion
  11.1 1.1 reduce-window.6
  12.2 0.2 slice_reduce_fusion
  12.5 0.2 fusion.16
  12.8 1.1 copy.33
  14.2 0.8 copy.39.weights
  15.1 0.7 fusion.10
  15.8 0.7 fusion.9
  16.6 1.0 fusion.14
  17.6 0.7 convolution_convert_fusion.part
  18.3 0.4 copy-done.1
  18.8 56.9 %front.1 = (bf16[8,96,2048]{2,1,0:T(8,128)(2,1)S(1)}, bf16[256,512]{1,0:T(8,128)(2,1)S(1)}) custom-call(bf16[256,2048]{1,0:T(8,128)(2,1)S(1)} %convolution_convert_fusion.part, bf16[256,2048]{1,0:T(8,128)(2,1)S(1)} %copy-done.1, f32[1,2048]{1,0:T(1,128)S(1)} %bitcast.56, s32[2,256]{1,0:T(2,128)S(1)} %copy.38.slots_row), custom_call_target="tpu_custom_call" | custom-call | tf_op jit(solution)/shard_map/front/pallas_call | solution.py:329
  75.7 3.5 %fusion.2 = f32[768,1024]{1,0:T(8,128)S(1)} fusion(bf16[768,2048]{1,0:T(8,128)(2,1)S(1)} %bitcast.57, bf16[1,2048,1024]{2,1,0:T(8,128)(2,1)S(1)} %copy-done.4), kind=kOutput, calls=%fused_computation.2 | convolution fusion | flops 3221225472 | bytes 10485760 | tf_op jit(solution)/shard_map/dot_general | solution.py:358
  79.2 3.8 %multiply_convert_fusion = bf16[768,1024]{1,0:T(8,128)(2,1)S(1)} fusion(f32[768,1024]{1,0:T(8,128)S(1)} %fusion.2, bf16[768,2048]{1,0:T(8,128)(2,1)S(1)} %bitcast.58, bf16[1,2048,1024]{2,1,0:T(8,128)(2,1)S(1)} %copy-done.5), kind=kOutput, calls=%fused_computation.8 | convolution fusion | flops 3225944064 | bytes 12058624 | tf_op jit(solution)/shard_map/dot_general | solution.py:357
  83.0 3.8 %fusion.6 = bf16[768,2048]{1,0:T(8,128)(2,1)S(1)} fusion(bf16[768,1024]{1,0:T(8,128)(2,1)S(1)} %multiply_convert_fusion, bf16[1,1024,2048]{2,1,0:T(8,128)(2,1)S(1)} %copy-done.6), kind=kOutput, calls=%fused_computation.6 | convolution fusion | flops 3222798336 | bytes 8912896 | tf_op jit(solution)/shard_map/dot_general | solution.py:360
  86.9 45.4 %back.1 = bf16[64,2048]{1,0:T(8,128)(2,1)S(1)} custom-call(bf16[8,96,2048]{2,1,0:T(8,128)(2,1)S(1)} %bitcast.54, s32[256,2]{1,0:T(8,128)S(1)} %add.51.slots, f32[256,2]{1,0:T(8,128)S(1)} %copy.39.weights, bf16[256,512]{1,0:T(8,128)(2,1)S(1)} %get-tuple-element.8.stream), custom_call_target="tpu_custom_call" | custom-call | tf_op jit(solution)/shard_map/back/pallas_call | solution.py:362
  132.3 0.7 copy.44
  (32 shorter events, 0.9 us)
Async XLA Ops:
  0.0 17.6 %copy-start = (bf16[512,2048]{1,0:T(8,128)(2,1)S(1)}, bf16[512,2048]{1,0:T(8,128)(2,1)}, u32[]{:S(2)}) copy-start(bf16[512,2048]{1,0:T(8,128)(2,1)} %param.16) | copy-start | bytes 6291460
  0.0 15.7 %copy-start.3 = (f32[8]{0:T(128)S(1)}, f32[8]{0:T(128)}, u32[]{:S(2)}) copy-start(f32[8]{0:T(128)} %param.15) | copy-start | bytes 100
  1.2 13.9 %collective-permute-start.1 = (bf16[128,64]{0,1:T(8,128)(2,1)S(1)}, bf16[128,64]{0,1:T(8,128)(2,1)S(1)}, u32[]{:S(2)}, u32[]{:S(2)}) collective-permute-start(bf16[128,64]{0,1:T(8,128)(2,1)S(1)} %slice.17), channel_id=1, source_target_pairs={{0,4},{4,8},{8,12},{12,16},{16,20},{20,24},{24,28},{1,5},{5,9},{9,... | collective-permute-start | bytes 49160 | tf_op jit(solution)/shard_map/ppermute | solution.py:21
  4.7 11.9 %collective-permute-start = (bf16[128,64]{0,1:T(8,128)(2,1)S(1)}, bf16[128,64]{0,1:T(8,128)(2,1)S(1)}, u32[]{:S(2)}, u32[]{:S(2)}) collective-permute-start(bf16[128,64]{0,1:T(8,128)(2,1)S(1)} %slice.16), channel_id=1, source_target_pairs={{0,4},{4,8},{8,12},{12,16},{16,20},{20,24},{24,28},{1,5},{5,9},{9,... | collective-permute-start | bytes 49160 | tf_op jit(solution)/shard_map/ppermute | solution.py:21
  17.6 1.2 copy-start.1
  17.6 1.2 copy-start.2
  17.6 58.1 %copy-start.4 = (bf16[1,2048,1024]{2,1,0:T(8,128)(2,1)S(1)}, bf16[1,2048,1024]{2,1,0:T(8,128)(2,1)}, u32[]{:S(2)}) copy-start(bf16[1,2048,1024]{2,1,0:T(8,128)(2,1)} %param.22) | copy-start | bytes 12582916
  75.7 3.5 %copy-start.5 = (bf16[1,2048,1024]{2,1,0:T(8,128)(2,1)S(1)}, bf16[1,2048,1024]{2,1,0:T(8,128)(2,1)}, u32[]{:S(2)}) copy-start(bf16[1,2048,1024]{2,1,0:T(8,128)(2,1)} %param.21) | copy-start | bytes 12582916
  79.2 3.8 %copy-start.6 = (bf16[1,1024,2048]{2,1,0:T(8,128)(2,1)S(1)}, bf16[1,1024,2048]{2,1,0:T(8,128)(2,1)}, u32[]{:S(2)}) copy-start(bf16[1,1024,2048]{2,1,0:T(8,128)(2,1)} %param.23) | copy-start | bytes 12582916

commit v2 on v0

v2 whole, which is shorter than its diff:
```python
import functools

import jax
import jax.numpy as jnp
from jax import lax
from jax.experimental import pallas as pl
from jax.experimental.pallas import tpu as pltpu
from jax.sharding import PartitionSpec as P

HEAD_DIM = 64
REP = 8
WINDOW = 128
MESH = pl.DeviceIdType.MESH

norm_eps = 1e-06


def slot_targets(routes, experts_n, slot_cap):
    flat_ids = routes.reshape(-1)
    onehot = (flat_ids[:, None] == jnp.arange(experts_n, dtype=jnp.int32)[None, :]).astype(
        jnp.int32
    )
    before = jnp.cumsum(onehot, axis=0) - onehot
    targets = flat_ids * slot_cap + jnp.sum(before * onehot, axis=1)
    return targets.reshape(routes.shape)


def greet(n_sp, n_tp, sp, tp):
    barrier = pltpu.get_barrier_semaphore()
    for d in range(1, n_tp):
        pl.semaphore_signal(
            barrier, inc=1, device_id=(sp, lax.rem(tp + d, n_tp)), device_id_type=MESH
        )
    for d in range(1, n_sp):
        pl.semaphore_signal(
            barrier, inc=1, device_id=(lax.rem(sp + d, n_sp), tp), device_id_type=MESH
        )
    pl.semaphore_wait(barrier, n_tp + n_sp - 2)


def remote(src, dst, send, recv, device):
    return pltpu.make_async_remote_copy(
        src_ref=src,
        dst_ref=dst,
        send_sem=send,
        recv_sem=recv,
        device_id=device,
        device_id_type=MESH,
    )


GROUPS = 4


def layer_kernel(
    n_sp,
    n_tp,
    query,
    kv,
    sinks,
    gain,
    slots_row,
    slots,
    weights,
    out_w_hbm,
    stream_hbm,
    gate_hbm,
    up_hbm,
    down_hbm,
    out,
    halo,
    attended,
    out_w,
    stream_in,
    gate,
    up,
    down,
    part0,
    px0,
    py0,
    qx0,
    qy0,
    fx0,
    fy0,
    stream,
    squares,
    squares_in,
    outgoing,
    arrived,
    hidden,
    part,
    px,
    py,
    qx,
    qy,
    fx,
    fy,
    summed,
    returned,
    acc,
    joined,
    halo_sem,
    load_sem,
    rs_send,
    rs_recv,
    sq_send,
    sq_recv,
    a2a_send,
    a2a_recv,
    ag_send,
    ag_recv,
    ret_send,
    ret_recv,
    last_send,
    last_recv,
):
    sp = lax.axis_index("sp")
    tp = lax.axis_index("tp")
    relay = n_tp == 4
    tok, width = stream.shape
    depth = arrived.shape[2]
    cap = arrived.shape[1]
    top = slots.shape[1]
    rows = out.shape[0]
    size = n_sp // GROUPS
    half = width // 2
    ff = hidden.shape[1]
    across = tp + 1 - 2 * lax.rem(tp, 2)
    down_tp = lax.rem(tp + 2, n_tp)
    corner = lax.rem(across + 2, n_tp)
    f32 = jnp.float32
    bf16 = jnp.bfloat16

    def cols(p, part_of=None):
        if part_of is None:
            return pl.ds(pl.multiple_of(p * width, width), width)
        return pl.ds(pl.multiple_of(p * width + part_of * half, half), half)

    mine = cols(tp)
    loads = [
        pltpu.make_async_copy(out_w_hbm, out_w, load_sem.at[0]),
        pltpu.make_async_copy(stream_hbm.at[:, mine], stream_in, load_sem.at[1]),
        pltpu.make_async_copy(gate_hbm.at[0], gate, load_sem.at[2]),
        pltpu.make_async_copy(up_hbm.at[0], up, load_sem.at[3]),
        pltpu.make_async_copy(down_hbm.at[0], down, load_sem.at[4]),
    ]
    for c in loads:
        c.start()
    greet(n_sp, n_tp, sp, tp)
    sent = []

    def go(c):
        c.start()
        sent.append(c)
        return c

    tail = go(
        remote(
            kv.at[pl.ds(tok - WINDOW, WINDOW)],
            halo,
            halo_sem.at[0],
            halo_sem.at[1],
            (lax.rem(sp + 1, n_sp), tp),
        )
    )

    def reduce_first(src, lead, bufs, g):
        bx, by = bufs[0], bufs[1]
        pieces = []
        if relay:
            plan = (
                (1, corner, 0, bx.at[1], across),
                (3, corner, 1, by.at[1], down_tp),
                (0, across, 0, bx.at[0], across),
                (2, down_tp, 1, by.at[0], down_tp),
            )
            for i, owner, h, dst, to in plan:
                pieces.append(
                    go(
                        remote(
                            src.at[lead + (cols(owner, h),)],
                            dst,
                            rs_send.at[g, i],
                            rs_recv.at[g, i],
                            (sp, to),
                        )
                    )
                )
        else:
            for q in range(1, n_tp):
                peer = lax.rem(tp + q, n_tp)
                pieces.append(
                    go(
                        remote(
                            src.at[lead + (cols(peer),)],
                            bx.at[q - 1],
                            rs_send.at[g, q - 1],
                            rs_recv.at[g, q - 1],
                            (sp, peer),
                        )
                    )
                )
        return pieces

    def reduce_second(src, lead, bufs, g, pieces):
        if not relay:
            return
        bx, by, rx, ry, tx, ty = bufs
        pieces[0].wait_recv()
        ty[...] = (
            src[lead + (cols(down_tp, 0),)].astype(f32) + bx.at[1][...].astype(f32)
        ).astype(bf16)
        pieces[1].wait_recv()
        tx[...] = (
            src[lead + (cols(across, 1),)].astype(f32) + by.at[1][...].astype(f32)
        ).astype(bf16)
        pieces.append(go(remote(ty, ry, rs_send.at[g, 4], rs_recv.at[g, 4], (sp, down_tp))))
        pieces.append(go(remote(tx, rx, rs_send.at[g, 5], rs_recv.at[g, 5], (sp, across))))

    def reduce_last(src, lead, bufs, pieces):
        bx, by, rx, ry = bufs[:4]
        if not relay:
            total = src[lead + (mine,)].astype(f32)
            for q in range(1, n_tp):
                pieces[q - 1].wait_recv()
                total = total + bx.at[q - 1][...].astype(f32)
            return total
        pieces[2].wait_recv()
        pieces[4].wait_recv()
        first = src[lead + (cols(tp, 0),)].astype(f32) + bx.at[0][...].astype(f32)
        first = first + ry[...].astype(f32)
        pieces[3].wait_recv()
        pieces[5].wait_recv()
        second = src[lead + (cols(tp, 1),)].astype(f32) + by.at[0][...].astype(f32)
        second = second + rx[...].astype(f32)
        return jnp.concatenate([first, second], axis=-1)

    row_at = lax.broadcasted_iota(jnp.int32, (WINDOW, 2 * WINDOW), 0)
    col_at = lax.broadcasted_iota(jnp.int32, (WINDOW, 2 * WINDOW), 1)
    gap = row_at + WINDOW - col_at
    in_window = (gap >= 0) & (gap < WINDOW)
    blocks = list(range(1, tok // WINDOW)) + [0]
    for b in blocks:
        here = slice(b * WINDOW, (b + 1) * WINDOW)
        if b == 0:
            tail.wait_recv()
            prior = halo[...]
            allowed = in_window & (sp * tok - WINDOW + col_at >= 0)
        else:
            prior = kv[(b - 1) * WINDOW : b * WINDOW]
            allowed = in_window
        both = jnp.concatenate([prior, kv[here]], axis=0)
        keys, vals = both[:, :HEAD_DIM], both[:, HEAD_DIM:]
        for h in range(query.shape[1] // HEAD_DIM):
            lanes = slice(h * HEAD_DIM, (h + 1) * HEAD_DIM)
            scores = lax.dot_general(
                query[here, lanes], keys, (((1,), (1,)), ((), ())), preferred_element_type=f32
            ) * HEAD_DIM ** (-0.5)
            scores = jnp.where(allowed, scores, -1e30)
            sink = sinks[0:1, h : h + 1]
            peak = jnp.maximum(jnp.max(scores, axis=1, keepdims=True), sink)
            terms = jnp.exp(scores - peak)
            denom = jnp.sum(terms, axis=1, keepdims=True) + jnp.exp(sink - peak)
            probs = (terms / denom).astype(bf16)
            attended[here, lanes] = jnp.dot(probs, vals, preferred_element_type=f32).astype(bf16)
    loads[0].wait()
    for q in range(1, n_tp + 1):
        block = cols(lax.rem(tp + q, n_tp))
        part0[:, block] = jnp.dot(
            attended[...], out_w[:, block], preferred_element_type=f32
        ).astype(bf16)
    every = (slice(None),)
    bufs0 = (px0, py0, qx0, qy0, fx0, fy0)
    pieces = reduce_first(part0, every, bufs0, GROUPS)
    reduce_second(part0, every, bufs0, GROUPS, pieces)
    total = reduce_last(part0, every, bufs0, pieces)
    loads[1].wait()
    new_stream = (stream_in[...].astype(f32) + total).astype(bf16)
    values = new_stream.astype(f32)
    row_sum = jnp.sum(values * values, axis=1, keepdims=True)
    spread = jnp.transpose(jnp.broadcast_to(row_sum, (tok, 128)))
    squares[...] = spread[0:8]
    stream[...] = new_stream
    sq = []
    for d in range(1, n_tp):
        peer = lax.rem(tp + d, n_tp)
        sq.append(
            go(
                remote(
                    squares, squares_in.at[d - 1], sq_send.at[d - 1], sq_recv.at[d - 1], (sp, peer)
                )
            )
        )
    full = spread[0:8]
    for d in range(1, n_tp):
        sq[d - 1].wait_recv()
        full = full + squares_in[d - 1]
    scale = lax.rsqrt(full / depth + norm_eps)
    scale = jnp.transpose(jnp.broadcast_to(scale[0:1], (128, tok)))[:, 0:1]
    normed = (values * scale * gain[:, mine]).astype(bf16)

    def picked(j):
        want = lax.broadcasted_iota(jnp.int32, (cap, tok), 0) + j * cap
        hit = want == slots_row[0:1, :]
        for k in range(1, top):
            hit = hit | (want == slots_row[k : k + 1, :])
        onehot = jnp.where(hit, 1.0, 0.0).astype(bf16)
        return jnp.dot(onehot, normed, preferred_element_type=f32).astype(bf16)

    a2a = [None]
    for d in range(1, n_sp):
        j = lax.rem(sp + d, n_sp)
        outgoing[d - 1] = picked(j)
        a2a.append(
            remote(
                outgoing.at[d - 1],
                arrived.at[d, :, mine],
                a2a_send.at[d - 1],
                a2a_recv.at[d - 1],
                (j, tp),
            )
        )
        if d > 1:
            go(a2a[d - 1])
    arrived[0, :, mine] = picked(sp)
    go(a2a[-1])

    direct = {}

    def share(g, owner, part_of, i, to):
        block = arrived.at[pl.ds(g * size, size), :, cols(owner, part_of)]
        c = remote(block, block, ag_send.at[g, i], ag_recv.at[g, i], (sp, to))
        direct[g, i] = go(c)

    def gather_first(g):
        for d in range(g * size, (g + 1) * size):
            if d > 0:
                a2a[d].wait_recv()
        if relay:
            share(g, tp, None, 0, across)
            share(g, tp, None, 1, down_tp)
        else:
            for q in range(1, n_tp):
                share(g, tp, None, q - 1, lax.rem(tp + q, n_tp))

    def gather_second(g):
        if relay:
            direct[g, 0].wait_recv()
            share(g, across, 0, 2, down_tp)
            direct[g, 1].wait_recv()
            share(g, down_tp, 1, 3, across)

    def lead_of(g):
        return (pl.ds(g * size, size), slice(None))

    def bufs_of(g):
        return tuple(r.at[g] for r in (px, py, qx, qy, fx, fy))

    ff_tile = min(256, ff)

    def experts(g):
        for i in range(2 if relay else 0, 4 if relay else n_tp - 1):
            direct[g, i].wait_recv()
        if g == 0:
            for c in loads[2:]:
                c.wait()

        def inner(f, carry):
            lanes = pl.ds(pl.multiple_of(f * ff_tile, ff_tile), ff_tile)
            x = arrived[pl.ds(g * size, size)].reshape(size * cap, depth)
            gate_act = jnp.dot(x, gate[:, lanes], preferred_element_type=f32)
            up_act = jnp.dot(x, up[:, lanes], preferred_element_type=f32)
            hidden[:, lanes] = (jax.nn.silu(gate_act) * up_act).astype(bf16)
            return carry

        lax.fori_loop(0, ff // ff_tile, inner, 0)

        def outer(q, carry):
            block = cols(lax.rem(tp + 1 + q, n_tp))
            got = jnp.dot(hidden[...], down[:, block], preferred_element_type=f32).astype(bf16)
            part[pl.ds(g * size, size), :, block] = got.reshape(size, cap, width)
            return carry

        lax.fori_loop(0, n_tp, outer, 0)

    back = {}

    def send_back(g):
        total = reduce_last(part, lead_of(g), bufs_of(g), reduced[g]).astype(bf16)
        summed[pl.ds(g * size, size)] = total
        for d in range(g * size, (g + 1) * size):
            if d > 0:
                back[d] = go(
                    remote(
                        summed.at[d],
                        returned.at[d - 1],
                        ret_send.at[d - 1],
                        ret_recv.at[d - 1],
                        (lax.rem(sp + n_sp - d, n_sp), tp),
                    )
                )

    def take(g):
        for d in range(g * size, (g + 1) * size):
            if d > 0:
                back[d].wait_recv()
            block = returned[d - 1] if d > 0 else summed[0]
            expert = lax.rem(sp + d, n_sp)
            want = lax.broadcasted_iota(jnp.int32, (tok, cap), 1) + expert * cap
            gives = None if d == 0 else acc[...]
            for k in range(top):
                onehot = jnp.where(want == slots[:, k : k + 1], 1.0, 0.0).astype(bf16)
                term = jnp.dot(onehot, block, preferred_element_type=f32)
                term = term * weights[:, k : k + 1]
                gives = term if gives is None else gives + term
            acc[...] = gives

    reduced = {}
    for step in range(GROUPS + 5):
        if step < GROUPS:
            gather_first(step)
        if 1 <= step < GROUPS + 1:
            gather_second(step - 1)
        if 2 <= step < GROUPS + 2:
            g = step - 2
            experts(g)
            reduced[g] = reduce_first(part, lead_of(g), bufs_of(g), g)
        if 3 <= step < GROUPS + 3:
            g = step - 3
            reduce_second(part, lead_of(g), bufs_of(g), g, reduced[g])
        if 4 <= step < GROUPS + 4:
            send_back(step - 4)
        if 5 <= step:
            take(step - 5)

    joined[...] = (stream[...].astype(f32) + acc[...]).astype(bf16)
    last = []
    for q in range(1, n_tp):
        peer = lax.rem(tp + q, n_tp)
        there = pl.ds(pl.multiple_of(peer * rows, rows), rows)
        last.append(
            go(
                remote(
                    joined.at[there],
                    out.at[:, mine],
                    last_send.at[q - 1],
                    last_recv.at[q - 1],
                    (sp, peer),
                )
            )
        )
    out[:, mine] = joined[pl.ds(pl.multiple_of(tp * rows, rows), rows), :]
    for c in last:
        c.wait_recv()
    for c in sent:
        c.wait_send()


def vmem(count):
    return [pl.BlockSpec(memory_space=pltpu.VMEM)] * count


def per_device(
    query_rows,
    key_rows,
    value_rows,
    sink_logits,
    out_weight,
    stream_in,
    norm_gain,
    routes,
    route_weights,
    gate_weight,
    up_weight,
    down_weight,
):
    n_sp = lax.axis_size("sp")
    n_tp = lax.axis_size("tp")
    tok_count = query_rows.shape[0]
    local_heads = query_rows.shape[1] // HEAD_DIM
    tp_index = lax.axis_index("tp")
    kv_group = tp_index * local_heads // REP
    own_keys = lax.dynamic_slice_in_dim(key_rows, kv_group * HEAD_DIM, HEAD_DIM, 1)
    own_values = lax.dynamic_slice_in_dim(value_rows, kv_group * HEAD_DIM, HEAD_DIM, 1)
    kv = jnp.concatenate([own_keys, own_values], axis=1)
    depth = stream_in.shape[1]
    width = depth // n_tp
    half = width // 2
    row_share = tok_count // n_tp
    ff = gate_weight.shape[2]
    top_count = routes.shape[1]
    slot_cap = -(-3 * tok_count * top_count // (2 * n_sp) // 16) * 16
    targets = slot_targets(routes, n_sp, slot_cap)
    bf16 = jnp.bfloat16
    f32 = jnp.float32
    size = n_sp // GROUPS
    dma = pltpu.SemaphoreType.DMA
    buf = pltpu.VMEM
    if n_tp == 4:
        first0, first = (2, tok_count, half), (GROUPS, 2, size, slot_cap, half)
        second0, second = (tok_count, half), (GROUPS, size, slot_cap, half)
    else:
        first0 = (n_tp - 1, tok_count, width)
        first = (GROUPS, n_tp - 1, size, slot_cap, width)
        second0, second = (16, 128), (GROUPS, 16, 128)
    few = max(6, n_tp - 1)
    any_spec = pl.BlockSpec(memory_space=pl.ANY)
    return pl.pallas_call(
        functools.partial(layer_kernel, n_sp, n_tp),
        out_shape=jax.ShapeDtypeStruct((row_share, depth), bf16),
        in_specs=vmem(7) + [any_spec] * 5,
        out_specs=vmem(1)[0],
        scratch_shapes=[
            buf((WINDOW, 2 * HEAD_DIM), bf16),
            buf((tok_count, local_heads * HEAD_DIM), bf16),
            buf(out_weight.shape, bf16),
            buf((tok_count, width), bf16),
            buf((depth, ff), bf16),
            buf((depth, ff), bf16),
            buf((ff, depth), bf16),
            buf((tok_count, depth), bf16),
            buf(first0, bf16),
            buf(first0 if n_tp == 4 else second0, bf16),
            buf(second0, bf16),
            buf(second0, bf16),
            buf(second0, bf16),
            buf(second0, bf16),
            buf((tok_count, width), bf16),
            buf((8, tok_count), f32),
            buf((n_tp - 1, 8, tok_count), f32),
            buf((n_sp - 1, slot_cap, width), bf16),
            buf((n_sp, slot_cap, depth), bf16),
            buf((size * slot_cap, ff), bf16),
            buf((n_sp, slot_cap, depth), bf16),
            buf(first, bf16),
            buf(first if n_tp == 4 else second, bf16),
            buf(second, bf16),
            buf(second, bf16),
            buf(second, bf16),
            buf(second, bf16),
            buf((n_sp, slot_cap, width), bf16),
            buf((n_sp - 1, slot_cap, width), bf16),
            buf((tok_count, width), f32),
            buf((tok_count, width), bf16),
            dma((2,)),
            dma((5,)),
            dma((GROUPS + 1, few)),
            dma((GROUPS + 1, few)),
            dma((n_tp - 1,)),
            dma((n_tp - 1,)),
            dma((n_sp - 1,)),
            dma((n_sp - 1,)),
            dma((GROUPS, few)),
            dma((GROUPS, few)),
            dma((n_sp - 1,)),
            dma((n_sp - 1,)),
            dma((n_tp - 1,)),
            dma((n_tp - 1,)),
        ],
        compiler_params=pltpu.CompilerParams(
            collective_id=0, has_side_effects=True, vmem_limit_bytes=58 << 20
        ),
        name="layer",
    )(
        query_rows,
        kv,
        sink_logits.reshape(1, local_heads),
        norm_gain.reshape(1, depth),
        jnp.transpose(targets),
        targets,
        route_weights,
        out_weight,
        stream_in,
        gate_weight,
        up_weight,
        down_weight,
    )


def solution(mesh):
    return jax.shard_map(
        per_device,
        mesh=mesh,
        in_specs=(
            P("sp", "tp"),
            P("sp", None),
            P("sp", None),
            P("tp"),
            P("tp", None),
            P("sp", None),
            P(),
            P("sp", None),
            P("sp", None),
            P("sp", None, "tp"),
            P("sp", None, "tp"),
            P("sp", "tp", None),
        ),
        out_specs=P(("sp", "tp"), None),
        check_vma=False,
    )
```

time: 301 us -> 113 us (0.38)
  waiting for transfers between devices: 185 us -> 0 us
  Pallas kernels: 0 us -> 103 us
  blocking collectives: 25.5 us -> 0 us
  local copies, waits for them, and re-layouts: 27.1 us -> 6.39 us
  matrix products: 18.3 us -> 0 us
  other arithmetic: 18.3 us -> 2.69 us
  between operations: 13.4 us -> 0.08 us
  starting transfers between devices: 12 us -> 0 us
    pallas_call x0 -> x1, Pallas kernels: none -> 103 us  [per_device(): pl.pallas_call(functools.partial(layer_kernel, n_sp, n_tp), out_shape=jax...]
    all_to_all x1 -> x0, waiting for transfers between devices: 71.2 us -> none  [per_device(): lax.all_to_all(partial_value, 'sp', split_axis=0, concat_axis=0, tiled=True)]
    psum x1 -> x0, waiting for transfers between devices: 46.2 us -> none  [per_device(): lax.psum(jnp.dot(attended, out_weight, preferred_element_type=jnp.float32...]
    all_gather x1 -> x0, waiting for transfers between devices: 41.8 us -> none  [per_device(): arrived = lax.all_gather(arrived, 'tp', axis=2, tiled=True)]
    reduce_scatter x1 -> x0, waiting for transfers between devices: 26 us -> none  [per_device(): lax.psum_scatter(jnp.sum(chosen.reshape(row_share * lax.axis_size('tp'),...]
    all_to_all x1 -> x0, blocking collectives: 25.5 us -> none  [per_device(): lax.all_to_all(outgoing, 'sp', split_axis=0, concat_axis=0, tiled=True)]
    dot_general x6 -> x0, matrix products: 18.3 us -> none  [the longest x1 6.28 us: per_device(): jnp.dot(flat_rows, up_weight[0], preferred_element_type=jnp.float32)]
    reduce_sum x4 -> x1, other arithmetic: 12.7 us -> 0.09 us  [slot_targets(): targets = flat_ids * slot_cap + jnp.sum(before * onehot, axis=1)]
  transfers between devices with their start and end apart: 6 -> 0, of which waited for: 4 -> 0; matrix products, arithmetic and copies ran while one was open for 4% -> 0% of each run, Pallas kernels for 0% -> 0%
where the time goes in v2:
time: 113 us
  Pallas kernels  103 us (91%)
  local copies, waits for them, and re-layouts  6.39 us (6%)
  other arithmetic  2.69 us (2%)
    pallas_call x1, Pallas kernels, per_device(): pl.pallas_call(functools.partial(layer_kernel, n_sp, n_tp), out_shape=jax...  103 us
    unnamed x5, local copies, waits for them, and re-layouts  3.96 us

profile of v2, /device:TPU:0, one launch (start us, length us, event | category | flops | bytes accessed | tf_op | source)
XLA Modules:
  0.0 112.6 jit_solution(1045971904973340911)
XLA Ops:
  0.0 0.7 broadcast_multiply_fusion
  0.7 0.1 copy.25
  0.8 1.0 constant_dynamic-slice_fusion
  1.8 0.7 pad_maximum_fusion.kv
  2.5 0.8 copy.23
  3.3 0.1 eq.29
  3.5 0.1 eq.25
  3.6 1.1 %reduce-window.6 = s32[8,4,128]{2,0,1:T(8,128)S(1)} reduce-window(s32[8,4,128]{2,0,1:T(8,128)S(1)} %fusion.2, s32[]{:T(128)} %constant.22.clone.1), window={size=1x1x128 pad=0_0x0_0x127_0}, to_apply=%region_0.1 | reduce-window | flops 520192 | bytes 32772 | tf_op jit(solution)/shard_map/reduce-window
  4.8 0.2 slice_reduce_fusion
  5.0 0.1 fusion.1
  5.1 0.1 reduce_sum.12
  5.3 0.0 copy-start
  5.3 0.7 copy.26.slots_row
  6.0 1.5 %copy.27.weights = f32[256,2]{1,0:T(8,128)} copy(f32[256,2]{0,1:T(2,128)} %param.20) | data formatting | bytes 4096 | tf_op args[8]
  7.5 0.0 copy-done
  7.5 103.4 %layer.1 = bf16[64,2048]{1,0:T(8,128)(2,1)} custom-call(bf16[256,512]{1,0:T(8,128)(2,1)} %query.1, bf16[256,128]{1,0:T(8,128)(2,1)} %pad_maximum_fusion.kv, f32[1,8]{1,0:T(1,128)} %bitcast.13, f32[1,2048]{1,0:T(1,128)} %bitcast.12, s32[2,256]{1,0:T(2,128)} %copy.26.slots_row, s32[256,2]{1,0:T(8,128)} %copy-done, f32[256,2]{1,0:T(8,128)} %copy.27.weights, ...), custom_call_target="tpu_custom_call" | custom-call | tf_op jit(solution)/shard_map/layer/pallas_call | solution.py:508
  110.9 1.7 %copy.29 = bf16[64,2048]{1,0:T(8,128)(2,1)} copy(bf16[64,2048]{1,0:T(8,128)(2,1)} %layer.1) | data formatting | bytes 524288
  (4 shorter events, 0.1 us)
Async XLA Ops:
  5.3 2.2 %copy-start = (s32[256,2]{1,0:T(8,128)}, s32[256,2]{1,0:T(8,128)S(1)}, u32[]{:S(2)}) copy-start(s32[256,2]{1,0:T(8,128)S(1)} %add.10.slots) | copy-start | bytes 6148

commit v3 on v2

--- a/solution.py
+++ b/solution.py
@@ -13,16 +13,6 @@
 MESH = pl.DeviceIdType.MESH
 
 norm_eps = 1e-06
-
-
-def slot_targets(routes, experts_n, slot_cap):
-    flat_ids = routes.reshape(-1)
-    onehot = (flat_ids[:, None] == jnp.arange(experts_n, dtype=jnp.int32)[None, :]).astype(
-        jnp.int32
-    )
-    before = jnp.cumsum(onehot, axis=0) - onehot
-    targets = flat_ids * slot_cap + jnp.sum(before * onehot, axis=1)
-    return targets.reshape(routes.shape)
 
 
 def greet(n_sp, n_tp, sp, tp):
@@ -56,12 +46,12 @@
     n_sp,
     n_tp,
     query,
-    kv,
+    key_rows,
+    value_rows,
     sinks,
     gain,
-    slots_row,
-    slots,
-    weights,
+    routes,
+    route_weights,
     out_w_hbm,
     stream_hbm,
     gate_hbm,
@@ -120,7 +110,7 @@
     tok, width = stream.shape
     depth = arrived.shape[2]
     cap = arrived.shape[1]
-    top = slots.shape[1]
+    top = routes.shape[0]
     rows = out.shape[0]
     size = n_sp // GROUPS
     half = width // 2
@@ -154,15 +144,22 @@
         sent.append(c)
         return c
 
-    tail = go(
-        remote(
-            kv.at[pl.ds(tok - WINDOW, WINDOW)],
-            halo,
-            halo_sem.at[0],
-            halo_sem.at[1],
-            (lax.rem(sp + 1, n_sp), tp),
+    local_heads = query.shape[1] // HEAD_DIM
+    kv_group = tp * local_heads // REP
+    pair = pl.ds(pl.multiple_of(kv_group // 2 * 2 * HEAD_DIM, 2 * HEAD_DIM), 2 * HEAD_DIM)
+    odd = lax.rem(kv_group, 2) == 1
+    tails = [
+        go(
+            remote(
+                source.at[pl.ds(tok - WINDOW, WINDOW), pair],
+                halo.at[i],
+                halo_sem.at[0, i],
+                halo_sem.at[1, i],
+                (lax.rem(sp + 1, n_sp), tp),
+            )
         )
-    )
+        for i, source in enumerate((key_rows, value_rows))
+    ]
 
     def reduce_first(src, lead, bufs, g):
         bx, by = bufs[0], bufs[1]
@@ -235,23 +232,39 @@
         second = second + rx[...].astype(f32)
         return jnp.concatenate([first, second], axis=-1)
 
+    def lead0(b):
+        return (pl.ds(b * WINDOW, WINDOW),)
+
+    def bufs0(b):
+        return tuple(ref.at[b] for ref in (px0, py0, qx0, qy0, fx0, fy0))
+
     row_at = lax.broadcasted_iota(jnp.int32, (WINDOW, 2 * WINDOW), 0)
     col_at = lax.broadcasted_iota(jnp.int32, (WINDOW, 2 * WINDOW), 1)
     gap = row_at + WINDOW - col_at
     in_window = (gap >= 0) & (gap < WINDOW)
+
+    def own_head(both):
+        return jnp.where(odd, both[:, HEAD_DIM:], both[:, :HEAD_DIM])
+
+    begun = {}
+    waited = False
     blocks = list(range(1, tok // WINDOW)) + [0]
     for b in blocks:
         here = slice(b * WINDOW, (b + 1) * WINDOW)
         if b == 0:
-            tail.wait_recv()
-            prior = halo[...]
+            for c in tails:
+                c.wait_recv()
+            priors = (halo[0], halo[1])
             allowed = in_window & (sp * tok - WINDOW + col_at >= 0)
         else:
-            prior = kv[(b - 1) * WINDOW : b * WINDOW]
+            before = slice((b - 1) * WINDOW, b * WINDOW)
+            priors = (key_rows[before, pair], value_rows[before, pair])
             allowed = in_window
-        both = jnp.concatenate([prior, kv[here]], axis=0)
-        keys, vals = both[:, :HEAD_DIM], both[:, HEAD_DIM:]
-        for h in range(query.shape[1] // HEAD_DIM):
+        keys, vals = (
+            own_head(jnp.concatenate([prior, source[here, pair]], axis=0))
+            for prior, source in zip(priors, (key_rows, value_rows))
+        )
+        for h in range(local_heads):
             lanes = slice(h * HEAD_DIM, (h + 1) * HEAD_DIM)
             scores = lax.dot_general(
                 query[here, lanes], keys, (((1,), (1,)), ((), ())), preferred_element_type=f32
@@ -263,17 +276,44 @@
             denom = jnp.sum(terms, axis=1, keepdims=True) + jnp.exp(sink - peak)
             probs = (terms / denom).astype(bf16)
             attended[here, lanes] = jnp.dot(probs, vals, preferred_element_type=f32).astype(bf16)
-    loads[0].wait()
-    for q in range(1, n_tp + 1):
-        block = cols(lax.rem(tp + q, n_tp))
-        part0[:, block] = jnp.dot(
-            attended[...], out_w[:, block], preferred_element_type=f32
-        ).astype(bf16)
-    every = (slice(None),)
-    bufs0 = (px0, py0, qx0, qy0, fx0, fy0)
-    pieces = reduce_first(part0, every, bufs0, GROUPS)
-    reduce_second(part0, every, bufs0, GROUPS, pieces)
-    total = reduce_last(part0, every, bufs0, pieces)
+        if not waited:
+            loads[0].wait()
+            waited = True
+        for q in range(1, n_tp + 1):
+            block = cols(lax.rem(tp + q, n_tp))
+            part0[here, block] = jnp.dot(
+                attended[here], out_w[:, block], preferred_element_type=f32
+            ).astype(bf16)
+        begun[b] = reduce_first(part0, lead0(b), bufs0(b), n_sp + b)
+
+    expert_at = lax.broadcasted_iota(jnp.int32, (n_sp, tok), 0)
+    members = [
+        jnp.where(routes[k : k + 1, :] == expert_at, 1.0, 0.0).astype(f32) for k in range(top)
+    ]
+    earlier = jnp.where(
+        lax.broadcasted_iota(jnp.int32, (tok, tok), 0)
+        < lax.broadcasted_iota(jnp.int32, (tok, tok), 1),
+        1.0,
+        0.0,
+    ).astype(bf16)
+    rank = jnp.dot(sum(members).astype(bf16), earlier, preferred_element_type=f32)
+    slots_row = [
+        routes[k : k + 1, :].astype(f32) * cap
+        + jnp.sum(rank * members[k], axis=0, keepdims=True)
+        for k in range(top)
+    ]
+
+    def upright(row):
+        return jnp.transpose(jnp.broadcast_to(row, (128, tok)))[:, 0:1]
+
+    slots = [upright(row) for row in slots_row]
+    weights = [upright(route_weights[k : k + 1, :]) for k in range(top)]
+
+    for b in blocks:
+        reduce_second(part0, lead0(b), bufs0(b), n_sp + b, begun[b])
+    total = jnp.concatenate(
+        [reduce_last(part0, lead0(b), bufs0(b), begun[b]) for b in sorted(blocks)], axis=0
+    )
     loads[1].wait()
     new_stream = (stream_in[...].astype(f32) + total).astype(bf16)
     values = new_stream.astype(f32)
@@ -296,17 +336,45 @@
         sq[d - 1].wait_recv()
         full = full + squares_in[d - 1]
     scale = lax.rsqrt(full / depth + norm_eps)
-    scale = jnp.transpose(jnp.broadcast_to(scale[0:1], (128, tok)))[:, 0:1]
+    scale = upright(scale[0:1])
     normed = (values * scale * gain[:, mine]).astype(bf16)
 
     def picked(j):
-        want = lax.broadcasted_iota(jnp.int32, (cap, tok), 0) + j * cap
-        hit = want == slots_row[0:1, :]
+        want = (lax.broadcasted_iota(jnp.int32, (cap, tok), 0) + j * cap).astype(f32)
+        hit = want == slots_row[0]
         for k in range(1, top):
-            hit = hit | (want == slots_row[k : k + 1, :])
+            hit = hit | (want == slots_row[k])
         onehot = jnp.where(hit, 1.0, 0.0).astype(bf16)
         return jnp.dot(onehot, normed, preferred_element_type=f32).astype(bf16)
 
+    direct = {}
+
+    def share(d, owner, part_of, i, to):
+        block = arrived.at[d, :, cols(owner, part_of)]
+        c = remote(block, block, ag_send.at[d, i], ag_recv.at[d, i], (sp, to))
+        direct[d, i] = go(c)
+
+    def gather_first(d):
+        if d > 0:
+            a2a[d].wait_recv()
+        if relay:
+            share(d, tp, None, 0, across)
+            share(d, tp, None, 1, down_tp)
+        else:
+            for q in range(1, n_tp):
+                share(d, tp, None, q - 1, lax.rem(tp + q, n_tp))
+
+    def gather_second(d):
+        if relay:
+            direct[d, 0].wait_recv()
+            share(d, across, 0, 2, down_tp)
+            direct[d, 1].wait_recv()
+            share(d, down_tp, 1, 3, across)
+
+    def group(g):
+        return range(g * size, (g + 1) * size)
+
+    arrived[0, :, mine] = picked(sp)
     a2a = [None]
     for d in range(1, n_sp):
         j = lax.rem(sp + d, n_sp)
@@ -322,36 +390,12 @@
         )
         if d > 1:
             go(a2a[d - 1])
-    arrived[0, :, mine] = picked(sp)
+        if d == 2:
+            gather_first(0)
     go(a2a[-1])
 
-    direct = {}
-
-    def share(g, owner, part_of, i, to):
-        block = arrived.at[pl.ds(g * size, size), :, cols(owner, part_of)]
-        c = remote(block, block, ag_send.at[g, i], ag_recv.at[g, i], (sp, to))
-        direct[g, i] = go(c)
-
-    def gather_first(g):
-        for d in range(g * size, (g + 1) * size):
-            if d > 0:
-                a2a[d].wait_recv()
-        if relay:
-            share(g, tp, None, 0, across)
-            share(g, tp, None, 1, down_tp)
-        else:
-            for q in range(1, n_tp):
-                share(g, tp, None, q - 1, lax.rem(tp + q, n_tp))
-
-    def gather_second(g):
-        if relay:
-            direct[g, 0].wait_recv()
-            share(g, across, 0, 2, down_tp)
-            direct[g, 1].wait_recv()
-            share(g, down_tp, 1, 3, across)
-
     def lead_of(g):
-        return (pl.ds(g * size, size), slice(None))
+        return (g, slice(None))
 
     def bufs_of(g):
         return tuple(r.at[g] for r in (px, py, qx, qy, fx, fy))
@@ -359,8 +403,9 @@
     ff_tile = min(256, ff)
 
     def experts(g):
-        for i in range(2 if relay else 0, 4 if relay else n_tp - 1):
-            direct[g, i].wait_recv()
+        for d in group(g):
+            for i in range(2 if relay else 0, 4 if relay else n_tp - 1):
+                direct[d, i].wait_recv()
         if g == 0:
             for c in loads[2:]:
                 c.wait()
@@ -385,51 +430,54 @@
 
     back = {}
 
-    def send_back(g):
-        total = reduce_last(part, lead_of(g), bufs_of(g), reduced[g]).astype(bf16)
-        summed[pl.ds(g * size, size)] = total
-        for d in range(g * size, (g + 1) * size):
-            if d > 0:
-                back[d] = go(
-                    remote(
-                        summed.at[d],
-                        returned.at[d - 1],
-                        ret_send.at[d - 1],
-                        ret_recv.at[d - 1],
-                        (lax.rem(sp + n_sp - d, n_sp), tp),
-                    )
+    def send_back(d):
+        total = reduce_last(part, lead_of(d), bufs_of(d), reduced[d])
+        summed[d] = total.astype(bf16)
+        if d > 0:
+            back[d] = go(
+                remote(
+                    summed.at[d],
+                    returned.at[d - 1],
+                    ret_send.at[d - 1],
+                    ret_recv.at[d - 1],
+                    (lax.rem(sp + n_sp - d, n_sp), tp),
                 )
+            )
 
     def take(g):
-        for d in range(g * size, (g + 1) * size):
+        for d in group(g):
             if d > 0:
                 back[d].wait_recv()
             block = returned[d - 1] if d > 0 else summed[0]
             expert = lax.rem(sp + d, n_sp)
-            want = lax.broadcasted_iota(jnp.int32, (tok, cap), 1) + expert * cap
+            want = (lax.broadcasted_iota(jnp.int32, (tok, cap), 1) + expert * cap).astype(f32)
             gives = None if d == 0 else acc[...]
             for k in range(top):
-                onehot = jnp.where(want == slots[:, k : k + 1], 1.0, 0.0).astype(bf16)
+                onehot = jnp.where(want == slots[k], 1.0, 0.0).astype(bf16)
                 term = jnp.dot(onehot, block, preferred_element_type=f32)
-                term = term * weights[:, k : k + 1]
+                term = term * weights[k]
                 gives = term if gives is None else gives + term
             acc[...] = gives
 
     reduced = {}
     for step in range(GROUPS + 5):
         if step < GROUPS:
-            gather_first(step)
+            for d in group(step):
+                if d > 0:
+                    gather_first(d)
         if 1 <= step < GROUPS + 1:
-            gather_second(step - 1)
+            for d in group(step - 1):
+                gather_second(d)
         if 2 <= step < GROUPS + 2:
-            g = step - 2
-            experts(g)
-            reduced[g] = reduce_first(part, lead_of(g), bufs_of(g), g)
+            experts(step - 2)
+            for d in group(step - 2):
+                reduced[d] = reduce_first(part, lead_of(d), bufs_of(d), d)
         if 3 <= step < GROUPS + 3:
-            g = step - 3
-            reduce_second(part, lead_of(g), bufs_of(g), g, reduced[g])
+            for d in group(step - 3):
+                reduce_second(part, lead_of(d), bufs_of(d), d, reduced[d])
         if 4 <= step < GROUPS + 4:
-            send_back(step - 4)
+            for d in group(step - 4):
+                send_back(d)
         if 5 <= step:
             take(step - 5)
 
@@ -478,11 +526,6 @@
     n_tp = lax.axis_size("tp")
     tok_count = query_rows.shape[0]
     local_heads = query_rows.shape[1] // HEAD_DIM
-    tp_index = lax.axis_index("tp")
-    kv_group = tp_index * local_heads // REP
-    own_keys = lax.dynamic_slice_in_dim(key_rows, kv_group * HEAD_DIM, HEAD_DIM, 1)
-    own_values = lax.dynamic_slice_in_dim(value_rows, kv_group * HEAD_DIM, HEAD_DIM, 1)
-    kv = jnp.concatenate([own_keys, own_values], axis=1)
     depth = stream_in.shape[1]
     width = depth // n_tp
     half = width // 2
@@ -490,19 +533,19 @@
     ff = gate_weight.shape[2]
     top_count = routes.shape[1]
     slot_cap = -(-3 * tok_count * top_count // (2 * n_sp) // 16) * 16
-    targets = slot_targets(routes, n_sp, slot_cap)
     bf16 = jnp.bfloat16
     f32 = jnp.float32
     size = n_sp // GROUPS
+    blocks = tok_count // WINDOW
     dma = pltpu.SemaphoreType.DMA
     buf = pltpu.VMEM
     if n_tp == 4:
-        first0, first = (2, tok_count, half), (GROUPS, 2, size, slot_cap, half)
-        second0, second = (tok_count, half), (GROUPS, size, slot_cap, half)
+        first0, first = (blocks, 2, WINDOW, half), (n_sp, 2, slot_cap, half)
+        second0, second = (blocks, WINDOW, half), (n_sp, slot_cap, half)
     else:
-        first0 = (n_tp - 1, tok_count, width)
-        first = (GROUPS, n_tp - 1, size, slot_cap, width)
-        second0, second = (16, 128), (GROUPS, 16, 128)
+        first0 = (blocks, n_tp - 1, WINDOW, width)
+        first = (n_sp, n_tp - 1, slot_cap, width)
+        second0, second = (blocks, 16, 128), (n_sp, 16, 128)
     few = max(6, n_tp - 1)
     any_spec = pl.BlockSpec(memory_space=pl.ANY)
     return pl.pallas_call(
@@ -511,7 +554,7 @@
         in_specs=vmem(7) + [any_spec] * 5,
         out_specs=vmem(1)[0],
         scratch_shapes=[
-            buf((WINDOW, 2 * HEAD_DIM), bf16),
+            buf((2, WINDOW, 2 * HEAD_DIM), bf16),
             buf((tok_count, local_heads * HEAD_DIM), bf16),
             buf(out_weight.shape, bf16),
             buf((tok_count, width), bf16),
@@ -542,16 +585,16 @@
             buf((n_sp - 1, slot_cap, width), bf16),
             buf((tok_count, width), f32),
             buf((tok_count, width), bf16),
-            dma((2,)),
+            dma((2, 2)),
             dma((5,)),
-            dma((GROUPS + 1, few)),
-            dma((GROUPS + 1, few)),
+            dma((n_sp + blocks, few)),
+            dma((n_sp + blocks, few)),
             dma((n_tp - 1,)),
             dma((n_tp - 1,)),
             dma((n_sp - 1,)),
             dma((n_sp - 1,)),
-            dma((GROUPS, few)),
-            dma((GROUPS, few)),
+            dma((n_sp, few)),
+            dma((n_sp, few)),
             dma((n_sp - 1,)),
             dma((n_sp - 1,)),
             dma((n_tp - 1,)),
@@ -563,12 +606,12 @@
         name="layer",
     )(
         query_rows,
-        kv,
+        key_rows,
+        value_rows,
         sink_logits.reshape(1, local_heads),
         norm_gain.reshape(1, depth),
-        jnp.transpose(targets),
-        targets,
-        route_weights,
+        jnp.transpose(routes),
+        jnp.transpose(route_weights),
         out_weight,
         stream_in,
         gate_weight,

time: 113 us -> 101 us (0.89)
  local copies, waits for them, and re-layouts: 6.39 us -> 1.67 us
  Pallas kernels: 103 us -> 99.1 us
  other arithmetic: 2.69 us -> 0 us
    pallas_call x1, Pallas kernels: 103 us -> 99.1 us  [per_device(): pl.pallas_call(functools.partial(layer_kernel, n_sp, n_tp), out_shape=jax...]
    unnamed x5 -> x1, local copies, waits for them, and re-layouts: 3.96 us -> 1.67 us
    another operation x2 -> x0, other arithmetic: 1.18 us -> none
where the time goes in v3:
time: 101 us
  Pallas kernels  99.1 us (98%)
  local copies, waits for them, and re-layouts  1.67 us (2%)
    pallas_call x1, Pallas kernels, per_device(): pl.pallas_call(functools.partial(layer_kernel, n_sp, n_tp), out_shape=jax...  99.1 us

profile of v3, /device:TPU:0, one launch (start us, length us, event | category | flops | bytes accessed | tf_op | source)
XLA Modules:
  0.0 100.8 jit_solution(9023958352107338853)
XLA Ops:
  0.0 99.1 %layer.1 = bf16[64,2048]{1,0:T(8,128)(2,1)} custom-call(bf16[256,512]{1,0:T(8,128)(2,1)} %query.1, bf16[256,256]{1,0:T(8,128)(2,1)} %key_rows.1, bf16[256,256]{1,0:T(8,128)(2,1)} %value_rows.1, f32[1,8]{1,0:T(1,128)} %bitcast.7, f32[1,2048]{1,0:T(1,128)} %bitcast.4, s32[2,256]{1,0:T(2,128)} %bitcast.5, f32[2,256]{1,0:T(2,128)} %bitcast.6, ...), custom_call_target="tpu_custom_call" | custom-call | tf_op jit(solution)/shard_map/layer/pallas_call | solution.py:551
  99.1 1.7 %copy.14 = bf16[64,2048]{1,0:T(8,128)(2,1)} copy(bf16[64,2048]{1,0:T(8,128)(2,1)} %layer.1) | data formatting | bytes 524288

commit v4 on v3

--- a/solution.py
+++ b/solution.py
@@ -374,10 +374,12 @@
     def group(g):
         return range(g * size, (g + 1) * size)
 
+    reach = [0, 1, n_sp - 1]
+    reach += sorted(range(2, n_sp - 1), key=lambda d: -min(d, n_sp - d))
     arrived[0, :, mine] = picked(sp)
     a2a = [None]
     for d in range(1, n_sp):
-        j = lax.rem(sp + d, n_sp)
+        j = lax.rem(sp + reach[d], n_sp)
         outgoing[d - 1] = picked(j)
         a2a.append(
             remote(
@@ -440,7 +442,7 @@
                     returned.at[d - 1],
                     ret_send.at[d - 1],
                     ret_recv.at[d - 1],
-                    (lax.rem(sp + n_sp - d, n_sp), tp),
+                    (lax.rem(sp + n_sp - reach[d], n_sp), tp),
                 )
             )
 
@@ -449,7 +451,7 @@
             if d > 0:
                 back[d].wait_recv()
             block = returned[d - 1] if d > 0 else summed[0]
-            expert = lax.rem(sp + d, n_sp)
+            expert = lax.rem(sp + reach[d], n_sp)
             want = (lax.broadcasted_iota(jnp.int32, (tok, cap), 1) + expert * cap).astype(f32)
             gives = None if d == 0 else acc[...]
             for k in range(top):

time: 101 us -> 99 us (0.980)
  Pallas kernels: 99.1 us -> 97.1 us
    pallas_call x1, Pallas kernels: 99.1 us -> 97.1 us  [per_device(): pl.pallas_call(functools.partial(layer_kernel, n_sp, n_tp), out_shape=jax...]
where the time goes in v4:
time: 99 us; the launch traced here: 98.8 us
  Pallas kernels  97.1 us (98%)
  local copies, waits for them, and re-layouts  1.67 us (2%)
    pallas_call x1, Pallas kernels, per_device(): pl.pallas_call(functools.partial(layer_kernel, n_sp, n_tp), out_shape=jax...  97.1 us

profile of v4, /device:TPU:0, one launch (start us, length us, event | category | flops | bytes accessed | tf_op | source)
XLA Modules:
  0.0 98.8 jit_solution(3636641580825318448)
XLA Ops:
  0.0 97.1 %layer.1 = bf16[64,2048]{1,0:T(8,128)(2,1)} custom-call(bf16[256,512]{1,0:T(8,128)(2,1)} %query.1, bf16[256,256]{1,0:T(8,128)(2,1)} %key_rows.1, bf16[256,256]{1,0:T(8,128)(2,1)} %value_rows.1, f32[1,8]{1,0:T(1,128)} %bitcast.7, f32[1,2048]{1,0:T(1,128)} %bitcast.4, s32[2,256]{1,0:T(2,128)} %bitcast.5, f32[2,256]{1,0:T(2,128)} %bitcast.6, ...), custom_call_target="tpu_custom_call" | custom-call | tf_op jit(solution)/shard_map/layer/pallas_call | solution.py:553
  97.1 1.7 %copy.14 = bf16[64,2048]{1,0:T(8,128)(2,1)} copy(bf16[64,2048]{1,0:T(8,128)(2,1)} %layer.1) | data formatting | bytes 524288
